TPU v7x, 32 devices: a whole 2x2x4 slice. The times are simulated.
32 devices in a mesh: sp: 4 (over y, x), tp: 8 (over z, core).
Axes of the slice: x: 2, y: 2, z: 4, core: 2. Of those that a mesh axis runs over, the one named last changes fastest.
Arguments:
- target: bfloat16 [512, 2048], P('sp'), may hold values from -6 to 6
- source: bfloat16 [1536, 2048], P('sp'), may hold values from -6 to 6
- cotangent: bfloat16 [512, 2048], P('sp'), may hold values from -192 to 192
- target_gain: float32 [2048], replicated, may hold values from 0.1 to 1.9
- source_gain: float32 [2048], replicated, may hold values from 0.1 to 1.9
- w_query: bfloat16 [2048, 4096], P(None, 'tp'), may hold values from -0.125 to 0.125
- w_key: bfloat16 [2048, 128], replicated, may hold values from -0.125 to 0.125
- w_value: bfloat16 [2048, 128], replicated, may hold values from -0.125 to 0.125
- w_out: bfloat16 [4096, 2048], P('tp'), may hold values from -0.09375 to 0.09375
Outputs:
- grad_target: bfloat16 [512, 2048], P(('sp', 'tp'))
- grad_source: bfloat16 [1536, 2048], P(('sp', 'tp'))
- grad_out_w: bfloat16 [4096, 2048], P('tp', 'sp')
All inputs are finite; a program needn't handle non-finite values.
Results may differ from a plain program's by a relative error of at most 0.025.
Values may be sent and summed in bfloat16 or wider, within the bound.
A program may use at most 64 MiB of HBM per device.

v0:
```python
import functools
import math

import jax
import jax.numpy as jnp
from jax import lax
from jax.experimental import pallas as pl
from jax.experimental.pallas import tpu as pltpu
from jax.sharding import PartitionSpec as P

HEAD = 128
NORM_EPS = 1e-06
CORES = 2
F32 = jnp.float32
BF16 = jnp.bfloat16
MESH = pl.DeviceIdType.MESH
NN = (((1,), (0,)), ((), ()))
NT = (((1,), (1,)), ((), ()))
TN = (((0,), (0,)), ((), ()))


def dot(a, b, dims=NN):
    return lax.dot_general(a, b, dims, preferred_element_type=F32)


def inv_rms_of(wide):
    return lax.rsqrt(jnp.mean(wide * wide, axis=1, keepdims=True) + NORM_EPS)


def norm_into(src, gain, dst, block, base, count):
    def body(i, _):
        rows = pl.ds(pl.multiple_of(base + i * block, block), block)
        wide = src[rows, :].astype(F32)
        dst[rows, :] = (wide * inv_rms_of(wide) * gain[...]).astype(BF16)
        return 0

    lax.fori_loop(0, count // block, body, 0)


def norm_back(wide, gain, upstream):
    inv = inv_rms_of(wide)
    unit = wide * inv
    pulled = upstream * gain
    return inv * (pulled - unit * jnp.mean(pulled * unit, axis=1, keepdims=True))


def own_rows(ref, place, rows):
    if rows % 16 == 0:
        return ref[pl.ds(pl.multiple_of(place * rows, 16), rows), :].astype(F32)
    padded = -(-rows // 16) * 16
    line = lax.broadcasted_iota(jnp.int32, (padded, ref.shape[0]), 0) + place * rows
    column = lax.broadcasted_iota(jnp.int32, (padded, ref.shape[0]), 1)
    pick = jnp.where(line == column, 1.0, 0.0).astype(BF16)
    return dot(pick, ref[...])[:rows]


def kernel(
    S, T,
    target_h, source_h, cot_h, tgain_h, sgain_h, wq_h, wk_h, wv_h, wo_h,
    gt_out, gs_out, go_out,
    target, source, cot, tgain, sgain, wq, wkv, wo, normed, kv, cotb, att, e_buf,
    kvg, kvg_in, red, red_in, red2, fin_in, pt, pt_in, ptr, ptr_in, stage,
    gt_ref, gs_ref, go_ref, load_sem, send, recv,
):
    Z = T // CORES
    me, t = lax.axis_index("sp"), lax.axis_index("tp")
    c, z = lax.rem(t, CORES), lax.div(t, CORES)
    sibling = {"sp": me, "tp": z * CORES + (1 - c)}
    TR, D = target.shape
    SG = source.shape[0]
    QW = wq.shape[1]
    H = QW // HEAD
    half = SG // 2
    thalf = TR // 2
    W = D // S
    SR, RR = SG // T, TR // T
    inv_root = HEAD ** (-0.5)

    X = math.isqrt(S) if math.isqrt(S) ** 2 == S else S
    Y = S // X
    steps = sorted(
        ((i // X, i % X) for i in range(S)), key=lambda yx: ((yx[0] > 0) + (yx[1] > 0), yx)
    )
    near = [d for d in range(1, S) if 0 in steps[d]]
    far = [d for d in range(1, S) if 0 not in steps[d]]

    def sp_place(d, way=1):
        dy, dx = steps[d]
        y = lax.rem(lax.div(me, X) + (dy if way > 0 else Y - dy), Y)
        x = lax.rem(lax.rem(me, X) + (dx if way > 0 else X - dx), X)
        return y * X + x

    def sp_peer(d, way=1):
        return {"sp": sp_place(d, way), "tp": t}

    def z_peer(d):
        return {"sp": me, "tp": lax.rem(z + d, Z) * CORES + c}

    sends = []

    def put(src, dst, lane, slot, who):
        copy = pltpu.make_async_remote_copy(
            src_ref=src, dst_ref=dst, send_sem=send.at[lane, slot], recv_sem=recv.at[lane, slot],
            device_id=who, device_id_type=MESH,
        )
        copy.start()
        sends.append(copy)
        return copy

    mine = pl.ds(pl.multiple_of(c * half, half), half)
    others = pl.ds(pl.multiple_of((1 - c) * half, half), half)
    pairs = (
        (source_h.at[mine], source.at[mine]), (wk_h, wkv.at[:, :HEAD]), (wv_h, wkv.at[:, HEAD:]),
        (target_h, target), (wq_h, wq), (cot_h, cot), (wo_h, wo),
        (sgain_h, sgain), (tgain_h, tgain), (source_h.at[others], source.at[others]),
    )
    loads = [pltpu.make_async_copy(a, b, load_sem.at[i]) for i, (a, b) in enumerate(pairs)]
    for i in (7, 0, 1, 2):
        loads[i].start()

    barrier = pltpu.get_barrier_semaphore()
    friends = [sibling] + [sp_peer(d) for d in range(1, S)] + [z_peer(d) for d in range(1, Z)]
    for who in friends:
        pl.semaphore_signal(barrier, inc=1, device_id=who, device_id_type=MESH)

    loads[7].wait()
    loads[0].wait()
    for i in (9, 3, 5, 8, 4, 6):
        loads[i].start()
    norm_into(source, sgain, normed, 32, c * half, half)
    loads[1].wait()
    loads[2].wait()
    kv[0, c] = dot(normed[mine, :], wkv[...]).astype(BF16)
    pl.semaphore_wait(barrier, len(friends))
    kv_put = [None] + [put(kv.at[0, c], kv.at[d, c], 0, d, sp_peer(d)) for d in range(1, S)]
    loads[5].wait()
    cot_put = [None]
    for d in range(1, S):
        columns = pl.ds(pl.multiple_of(sp_place(d) * W, 128), W)
        rows = pl.ds(pl.multiple_of(c * thalf, thalf), thalf)
        cot_put.append(put(cot.at[rows, columns], cotb.at[d, c], 1, d, sp_peer(d)))

    loads[9].wait()
    norm_into(source, sgain, normed, 32, (1 - c) * half, half)
    kv[0, 1 - c] = dot(normed[others, :], wkv[...]).astype(BF16)
    loads[8].wait()
    loads[3].wait()
    norm_into(target, tgain, normed, 32, 0, TR)
    loads[4].wait()
    query = dot(normed[:TR, :], wq[...]).astype(BF16)
    loads[6].wait()
    grad = dot(cot[...], wo[...], NT).astype(BF16)
    q_rows = jnp.concatenate([query[:, h * HEAD:(h + 1) * HEAD] for h in range(H)], axis=0)
    g_rows = jnp.concatenate([grad[:, h * HEAD:(h + 1) * HEAD] for h in range(H)], axis=0)

    def pair(d):
        both = jnp.concatenate([kv[d,0],kv[d,1]],axis=0)
        return both[:, :HEAD], both[:, HEAD:]

    def exponents(d):
        k, v = pair(d)
        e = jnp.exp2(dot(k, q_rows, NT) * (inv_root * math.log2(math.e)))
        e_buf[d] = e
        return jnp.sum(e, axis=0, keepdims=True), dot(v, e.astype(BF16), TN)

    total, out_t = exponents(0)
    kv_fwd = [None]
    for d in range(1, S):
        kv_put[d].wait_recv()
        kv_fwd.append(put(kv.at[d, c], kv.at[d, c], 2, d, sibling))
    for d in range(1, S):
        kv_fwd[d].wait_recv()
        more, out_more = exponents(d)
        total, out_t = total + more, out_t + out_more
    inv_total = 1.0 / total
    att_t = (out_t * inv_total).astype(BF16)
    att[0] = att_t
    delta = jnp.sum(att_t.astype(F32) * g_rows.astype(F32).T, axis=0, keepdims=True)
    att_put = {d: put(att.at[0], att.at[d], 3, d, sp_peer(d)) for d in near}

    def spread(d, grads):
        if SR % 8:
            stage[...] = grads
        for place in range(T):
            rows = slice(place * SR, (place + 1) * SR)
            block = stage[rows, :] if SR % 8 else grads[rows]
            kvg[place % CORES, d, place // CORES] = block.astype(BF16)

    def settle(d):
        kvg_put[d].wait_recv()
        red[d] = (kvg[c, d].astype(F32) + kvg_in[d].astype(F32)).astype(BF16)
        if d:
            return put(red.at[d], red_in.at[d], 5, d, sp_peer(d, -1))

    kvg_put = {}
    red_put = {}
    gq_t = None
    order = list(range(S - 1, -1, -1))
    for step, d in enumerate(order):
        k, v = pair(d)
        p = e_buf[d] * inv_total
        score_grad = (p * (dot(v, g_rows, NT) - delta)).astype(BF16)
        part = dot(k, score_grad, TN)
        gq_t = part if gq_t is None else gq_t + part
        k_grad = dot(score_grad, q_rows) * inv_root
        v_grad = dot(p.astype(BF16), g_rows)
        spread(d, jnp.concatenate([k_grad, v_grad], axis=1))
        kvg_put[d] = put(kvg.at[1 - c, d], kvg_in.at[d], 4, d, sibling)
        if step:
            red_put[order[step - 1]] = settle(order[step - 1])

    for d in far:
        att_put[d] = put(att.at[0], att.at[d], 3, d, sp_peer(d))
    gq_t = gq_t * inv_root
    gq = jnp.concatenate([gq_t[:, h * TR:(h + 1) * TR].T for h in range(H)], axis=1).astype(BF16)
    pulled = dot(gq, wq[...], NT)
    for place in range(T):
        if RR % 8:
            if place == 0:
                normed_rows = stage_rows(e_buf, pulled)
            block = normed_rows(place * RR, RR)
        else:
            block = pulled[place * RR:(place + 1) * RR]
        pt[place % CORES, place // CORES] = block.astype(BF16)
    pt_put = put(pt.at[1 - c], pt_in, 6, 0, sibling)
    settle(0)
    cot_fwd = [None]
    for d in range(1, S):
        cot_put[d].wait_recv()
        cot_fwd.append(put(cotb.at[d, c], cotb.at[d, c], 7, d, sibling))
    pt_put.wait_recv()
    ptr[...] = (pt[c].astype(F32) + pt_in[...].astype(F32)).astype(BF16)
    ptr_put = [None] + [
        put(ptr.at[lax.rem(z + d, Z)], ptr_in.at[d], 8, d, z_peer(d)) for d in range(1, Z)
    ]
    summed = red[0].astype(F32)
    for d in range(1, S):
        red_put[d].wait_recv()
        summed = summed + red_in[d].astype(F32)
    red2[...] = summed.astype(BF16)
    fin_put = [None] + [
        put(red2.at[lax.rem(z + d, Z)], fin_in.at[d], 9, d, z_peer(d)) for d in range(1, Z)
    ]

    att_all, cot_all = [att[0]], [cot[:, pl.ds(pl.multiple_of(me * W, 128), W)]]
    for d in range(1, S):
        att_put[d].wait_recv()
        cot_fwd[d].wait_recv()
        att_all.append(att[d])
        cot_all.append(jnp.concatenate([cotb[d,0],cotb[d,1]],axis=0))
    cot_rows = jnp.concatenate(cot_all, axis=0)
    for h in range(H):
        left = jnp.concatenate([a[:, h * TR:(h + 1) * TR] for a in att_all], axis=1)
        go_ref[h * HEAD:(h + 1) * HEAD, :] = dot(left, cot_rows).astype(BF16)

    writes = [
        pltpu.make_async_copy(a, b, load_sem.at[i])
        for i, (a, b) in enumerate(((go_ref, go_out), (gt_ref, gt_out), (gs_ref, gs_out)))
    ]
    writes[0].start()
    up = ptr[z].astype(F32)
    for d in range(1, Z):
        ptr_put[d].wait_recv()
        up = up + ptr_in[d].astype(F32)
    gt_ref[...] = norm_back(own_rows(target, t, RR), tgain[...], up).astype(BF16)
    writes[1].start()
    last = red2[z].astype(F32)
    for d in range(1, Z):
        fin_put[d].wait_recv()
        last = last + fin_in[d].astype(F32)
    up = dot(last.astype(BF16), wkv[...], NT)
    gs_ref[...] = norm_back(own_rows(source, t, SR), sgain[...], up).astype(BF16)
    writes[2].start()
    for copy in sends:
        copy.wait_send()
    for copy in writes:
        copy.wait()


def stage_rows(buf, rows):
    width = buf.shape[2]
    bands = rows.shape[1] // width
    for i in range(bands):
        buf[i, :rows.shape[0], :] = rows[:, i * width:(i + 1) * width]
    return lambda start, count: jnp.concatenate(
        [buf[i, start:start + count, :] for i in range(bands)], axis=1
    )


def on_device(S, T, target, source, cotangent, target_gain, source_gain, w_query, w_key, w_value, w_out):
    TR, D = target.shape
    SG = source.shape[0]
    QW = w_query.shape[1]
    R = QW // HEAD * TR
    Z = T // CORES
    SR, RR, W = SG // T, TR // T, D // S
    N = max(S, Z)
    hbm = pl.BlockSpec(memory_space=pltpu.HBM)
    V = pltpu.VMEM
    results = pl.pallas_call(
        functools.partial(kernel, S, T),
        out_shape=(
            jax.ShapeDtypeStruct((RR, D), BF16),
            jax.ShapeDtypeStruct((SR, D), BF16),
            jax.ShapeDtypeStruct((QW, W), BF16),
        ),
        in_specs=[hbm] * 9,
        out_specs=(hbm, hbm, hbm),
        scratch_shapes=[
            V((TR, D), BF16), V((SG, D), BF16), V((TR, D), BF16), V((1, D), F32), V((1, D), F32),
            V((D, QW), BF16), V((D, 2 * HEAD), BF16), V((QW, D), BF16),
            V((max(SG, TR), D), BF16),
            V((S, 2, SG // 2, 2 * HEAD), BF16), V((S, 2, TR // 2, W), BF16),
            V((S, HEAD, R), BF16), V((S, SG, R), F32),
            V((CORES, S, Z, SR, 2 * HEAD), BF16), V((S, Z, SR, 2 * HEAD), BF16),
            V((S, Z, SR, 2 * HEAD), BF16), V((S, Z, SR, 2 * HEAD), BF16),
            V((Z, SR, 2 * HEAD), BF16), V((Z, SR, 2 * HEAD), BF16),
            V((CORES, Z, RR, D), BF16), V((Z, RR, D), BF16), V((Z, RR, D), BF16), V((Z, RR, D), BF16),
            V((SG, 2 * HEAD), F32),
            V((RR, D), BF16), V((SR, D), BF16), V((QW, W), BF16),
            pltpu.SemaphoreType.DMA((10,)),
            pltpu.SemaphoreType.DMA((10, N)),
            pltpu.SemaphoreType.DMA((10, N)),
        ],
        compiler_params=pltpu.CompilerParams(
            collective_id=0, has_side_effects=True, vmem_limit_bytes=60 * 1024 * 1024
        ),
        name="attn_back",
    )(
        target, source, cotangent, target_gain.reshape(1, D), source_gain.reshape(1, D),
        w_query, w_key, w_value, w_out,
    )
    return pl.pallas_call(
        put_out,
        out_shape=tuple(jax.ShapeDtypeStruct(r.shape, r.dtype) for r in results),
        in_specs=[hbm, hbm, hbm],
        out_specs=(hbm, hbm, hbm),
        scratch_shapes=[V(r.shape, r.dtype) for r in results]
        + [pltpu.SemaphoreType.DMA((3,)), pltpu.SemaphoreType.DMA((3,))],
        compiler_params=pltpu.CompilerParams(vmem_limit_bytes=60 * 1024 * 1024),
        name="put_out",
    )(*results)


def put_out(a, b, c, a_out, b_out, c_out, a_mid, b_mid, c_mid, in_sem, out_sem):
    trios = ((a, a_mid, a_out), (b, b_mid, b_out), (c, c_mid, c_out))
    ins = [pltpu.make_async_copy(x, y, in_sem.at[i]) for i, (x, y, _) in enumerate(trios)]
    outs = [pltpu.make_async_copy(x, y, out_sem.at[i]) for i, (_, x, y) in enumerate(trios)]
    for copy in ins:
        copy.start()
    for before, after in zip(ins, outs):
        before.wait()
        after.start()
    for copy in outs:
        copy.wait()


def solution(mesh):
    in_specs = (
        P("sp", None), P("sp", None), P("sp", None), P(), P(),
        P(None, "tp"), P(), P(), P("tp", None),
    )
    out_specs = (P(("sp", "tp"), None), P(("sp", "tp"), None), P("tp", "sp"))
    return jax.shard_map(
        functools.partial(on_device, mesh.shape["sp"], mesh.shape["tp"]),
        mesh=mesh, in_specs=in_specs, out_specs=out_specs, check_vma=False,
    )
```

profile of v0, /device:TPU:0, one launch (start us, length us, event | category | flops | bytes accessed | tf_op | source)
XLA Modules:
  0.0 34.7 jit_solution(983048610215253377)
XLA Ops:
  0.6 32.0 %attn_back.1 = (bf16[16,2048]{1,0:T(8,128)(2,1)}, bf16[48,2048]{1,0:T(8,128)(2,1)}, bf16[512,512]{1,0:T(8,128)(2,1)}) custom-call(bf16[128,2048]{1,0:T(8,128)(2,1)} %target_h.1, bf16[384,2048]{1,0:T(8,128)(2,1)} %source_h.1, bf16[128,2048]{1,0:T(8,128)(2,1)} %cot_h.1, f32[1,2048]{1,0:T(1,128)} %bitcast.2, f32[1,2048]{1,0:T(1,128)} %bitcast.3, ...), custom_call_target="tpu_custom_call" | custom-call | tf_op jit(solution)/shard_map/attn_back/pallas_call | solution.py:300
  32.7 2.0 %put_out.1 = (bf16[16,2048]{1,0:T(8,128)(2,1)}, bf16[48,2048]{1,0:T(8,128)(2,1)}, bf16[512,512]{1,0:T(8,128)(2,1)}) custom-call(bf16[16,2048]{1,0:T(8,128)(2,1)} %get-tuple-element.6.a, bf16[48,2048]{1,0:T(8,128)(2,1)} %get-tuple-element.7.b, bf16[512,512]{1,0:T(8,128)(2,1)} %get-tuple-element.8.c), custom_call_target="tpu_custom_call" | custom-call | tf_op jit(solution)/shard_map/put_out/pallas_call | solution.py:333
where the time goes:
time: 34.9 us; the launch traced here: 34.7 us
  Pallas kernels  34 us (97%)
  between operations  0.64 us (2%)
    pallas_call x1, Pallas kernels, on_device(): pl.pallas_call(functools.partial(kernel, S, T), out_shape=(jax.ShapeDtype...  32 us
    pallas_call x1, Pallas kernels, on_device(): pl.pallas_call(put_out, out_shape=tuple((jax.ShapeDtypeStruct(r.shape, r....  2.02 us

commit v1 on v0

v1 whole, which is shorter than its diff:
```python
import functools
import math

import jax
import jax.numpy as jnp
from jax import lax
from jax.experimental import pallas as pl
from jax.experimental.pallas import tpu as pltpu
from jax.sharding import PartitionSpec as P

HEAD = 128
NORM_EPS = 1e-06
CORES = 2
F32 = jnp.float32
BF16 = jnp.bfloat16
MESH = pl.DeviceIdType.MESH
NN = (((1,), (0,)), ((), ()))
NT = (((1,), (1,)), ((), ()))
TN = (((0,), (0,)), ((), ()))


def dot(a, b, dims=NN):
    return lax.dot_general(a, b, dims, preferred_element_type=F32)


def inv_rms_of(wide):
    return lax.rsqrt(jnp.mean(wide * wide, axis=1, keepdims=True) + NORM_EPS)


def gained(src, gain, dst, rows):
    D = src.shape[1]
    step = 256
    squares = None
    for at in range(0, D, step):
        columns = slice(at, at + step)
        wide = src[rows, columns].astype(F32)
        dst[rows, columns] = (wide * gain[:, columns]).astype(BF16)
        part = wide * wide
        part = sum(part[:, i:i + 128] for i in range(0, step, 128))
        squares = part if squares is None else squares + part
    return lax.rsqrt(jnp.sum(squares, axis=1, keepdims=True) * (1.0 / D) + NORM_EPS)


def norm_back(wide, gain, upstream):
    inv = inv_rms_of(wide)
    unit = wide * inv
    pulled = upstream * gain
    return inv * (pulled - unit * jnp.mean(pulled * unit, axis=1, keepdims=True))


def own_rows(ref, place, rows):
    if rows % 16 == 0:
        return ref[pl.ds(pl.multiple_of(place * rows, 16), rows), :].astype(F32)
    padded = -(-rows // 16) * 16
    line = lax.broadcasted_iota(jnp.int32, (padded, ref.shape[0]), 0) + place * rows
    column = lax.broadcasted_iota(jnp.int32, (padded, ref.shape[0]), 1)
    pick = jnp.where(line == column, 1.0, 0.0).astype(BF16)
    return dot(pick, ref[...])[:rows]


def kernel(
    S, T,
    target_h, source_h, cot_h, tgain_h, sgain_h, wq_h, wk_h, wv_h, wo_h,
    gt_ref, gs_ref, go_ref,
    target, source, cot, tgain, sgain, wq, wkv, wo, normed, kv, cotb, att, e_buf, pg_buf,
    kvg, kvg_in, red, red_in, red2, fin_in, pt, pt_in, ptr, ptr_in, stage, wide_stage,
    load_sem, send, recv,
):
    Z = T // CORES
    me, t = lax.axis_index("sp"), lax.axis_index("tp")
    c, z = lax.rem(t, CORES), lax.div(t, CORES)
    sibling = {"sp": me, "tp": z * CORES + (1 - c)}
    TR, D = target.shape
    SG = source.shape[0]
    QW = wq.shape[1]
    H = QW // HEAD
    half = SG // 2
    thalf = TR // 2
    W = D // S
    SR, RR = SG // T, TR // T
    inv_root = HEAD ** (-0.5)
    parts = next(n for n in (3, 2, 1) if half % (16 * n) == 0)
    chunk = half // parts

    X = math.isqrt(S) if math.isqrt(S) ** 2 == S else S
    Y = S // X
    steps = sorted(
        ((i // X, i % X) for i in range(S)), key=lambda yx: ((yx[0] > 0) + (yx[1] > 0), yx)
    )
    near = [d for d in range(1, S) if 0 in steps[d]]
    far = [d for d in range(1, S) if 0 not in steps[d]]

    def sp_place(d, way=1):
        dy, dx = steps[d]
        y = lax.rem(lax.div(me, X) + (dy if way > 0 else Y - dy), Y)
        x = lax.rem(lax.rem(me, X) + (dx if way > 0 else X - dx), X)
        return y * X + x

    def sp_peer(d, way=1):
        return {"sp": sp_place(d, way), "tp": t}

    def z_peer(d):
        return {"sp": me, "tp": lax.rem(z + d, Z) * CORES + c}

    sends = []

    def put(src, dst, who):
        lane = len(sends)
        copy = pltpu.make_async_remote_copy(
            src_ref=src, dst_ref=dst, send_sem=send.at[lane], recv_sem=recv.at[lane],
            device_id=who, device_id_type=MESH,
        )
        copy.start()
        sends.append(copy)
        return copy

    def own_half(i):
        return pl.ds(pl.multiple_of(c * half + i * chunk, chunk), chunk)

    others = pl.ds(pl.multiple_of((1 - c) * half, half), half)
    pairs = [
        (sgain_h, sgain), (source_h.at[own_half(0)], source.at[own_half(0)]),
        (wk_h, wkv.at[:, :HEAD]), (wv_h, wkv.at[:, HEAD:]),
        (tgain_h, tgain), (target_h, target), (wq_h, wq), (cot_h, cot), (wo_h, wo),
        (source_h.at[others], source.at[others]),
    ] + [(source_h.at[own_half(i)], source.at[own_half(i)]) for i in range(1, parts)]
    loads = [pltpu.make_async_copy(a, b, load_sem.at[i]) for i, (a, b) in enumerate(pairs)]
    for i in (0, 1, 2, 3, *range(10, 9 + parts)):
        loads[i].start()

    barrier = pltpu.get_barrier_semaphore()
    friends = [sibling] + [sp_peer(d) for d in range(1, S)] + [z_peer(d) for d in range(1, Z)]
    for who in friends:
        pl.semaphore_signal(barrier, inc=1, device_id=who, device_id_type=MESH)

    kv_put = {d: [] for d in range(1, S)}
    for i in range(parts):
        if i == 0:
            loads[0].wait()
            loads[1].wait()
            for j in (5, 4, 7, 6, 8, 9):
                loads[j].start()
        else:
            loads[9 + i].wait()
        inv = gained(source, sgain, normed, own_half(i))
        if i == 0:
            loads[2].wait()
            loads[3].wait()
        rows = pl.ds(i * chunk, chunk)
        kv[0, c, rows, :] = (dot(normed[own_half(i), :], wkv[...]) * inv).astype(BF16)
        if i == 0:
            pl.semaphore_wait(barrier, len(friends))
        for d in far + near:
            kv_put[d].append(put(kv.at[0, c, rows], kv.at[d, c, rows], sp_peer(d)))
    kv_twin = put(kv.at[0, c], kv.at[0, c], sibling)
    loads[5].wait()
    loads[4].wait()
    inv = gained(target, tgain, normed, slice(0, TR))
    loads[6].wait()
    query = dot(normed[:TR, :], wq[...]) * inv
    loads[7].wait()
    loads[8].wait()
    grad = dot(cot[...], wo[...], NT)
    split = [slice(h * HEAD, (h + 1) * HEAD) for h in range(H)]
    q_rows = jnp.concatenate([query[:, h] for h in split], axis=0).astype(BF16)
    g_rows = jnp.concatenate([grad[:, h] for h in split], axis=0).astype(BF16)
    q_cols = jnp.concatenate([query[:, h].T for h in split], axis=1).astype(BF16)
    g_cols = jnp.concatenate([grad[:, h].T for h in split], axis=1).astype(BF16)

    def forward(blocks):
        both = jnp.concatenate([kv[d, part] for d, part in blocks], axis=0)
        k, v = both[:, :HEAD], both[:, HEAD:]
        e = jnp.exp2(dot(k, q_cols) * (inv_root * math.log2(math.e)))
        prob_grad = dot(v, g_cols)
        for i, (d, part) in enumerate(blocks):
            e_buf[d, part] = e[i * half:(i + 1) * half]
            pg_buf[d, part] = prob_grad[i * half:(i + 1) * half]
        tilted = (e * prob_grad).astype(BF16)
        return jnp.sum(e, axis=0, keepdims=True), dot(both, e.astype(BF16), TN), dot(k, tilted, TN)

    def more(state, blocks):
        return tuple(a + b for a, b in zip(state, forward(blocks)))

    kv_fwd = {}

    def hand_on(places):
        for d in places:
            for copy in kv_put[d]:
                copy.wait_recv()
            kv_fwd[d] = put(kv.at[d, c], kv.at[d, c], sibling)

    loads[9].wait()
    kv_twin.wait_recv()
    state = forward([(0, c), (0, 1 - c)])
    hand_on(near + far)
    cot_put = [None]
    for d in range(1, S):
        columns = pl.ds(pl.multiple_of(sp_place(d) * W, 128), W)
        rows = pl.ds(pl.multiple_of(c * thalf, thalf), thalf)
        cot_put.append(put(cot.at[rows, columns], cotb.at[d, c], sp_peer(d)))

    state = more(state, [(d, c) for d in near + far])
    for d in near + far:
        kv_fwd[d].wait_recv()
    state = more(state, [(d, 1 - c) for d in near + far])
    total, weighted, tilted_sum = state
    inv_total = 1.0 / total
    att_t = (weighted[HEAD:] * inv_total).astype(BF16)
    att[0] = att_t
    top, bottom = pl.ds(0, HEAD // 2), pl.ds(HEAD // 2, HEAD // 2)
    att_put = {d: [] for d in range(1, S)}
    for d in near:
        att_put[d].append(put(att.at[0, top], att.at[d, top], sp_peer(d)))
    delta = jnp.sum(att_t.astype(F32) * g_cols.astype(F32), axis=0, keepdims=True)

    def spread(d, grads):
        if SR % 8:
            stage[...] = grads
        for place in range(T):
            rows = slice(place * SR, (place + 1) * SR)
            block = stage[rows, :] if SR % 8 else grads[rows]
            kvg[place % CORES, d, place // CORES] = block.astype(BF16)

    kvg_put = {}
    red_put = {}
    pieces = [1, 2, 3, 0] if Z == 4 else [None]

    def backward(d):
        p = e_buf[d].reshape(SG, -1) * inv_total
        score_grad = (p * (pg_buf[d].reshape(SG, -1) - delta)).astype(BF16)
        k_grad = dot(score_grad, q_rows) * inv_root
        v_grad = dot(p.astype(BF16), g_rows)
        spread(d, jnp.concatenate([k_grad, v_grad], axis=1))
        kvg_put[d] = put(kvg.at[1 - c, d], kvg_in.at[d], sibling)

    def settle(d):
        kvg_put[d].wait_recv()
        red[d] = (kvg[c, d].astype(F32) + kvg_in[d].astype(F32)).astype(BF16)
        if d:
            red_put[d] = []
            for j in pieces:
                at = pl.ds(0, Z) if j is None else pl.ds(lax.rem(z + j, Z), 1)
                red_put[d].append(put(red.at[d, at], red_in.at[d, at], sp_peer(d, -1)))

    order = list(range(S - 1, -1, -1))
    backward(order[0])
    gq_t = (tilted_sum - delta * weighted[:HEAD]) * (inv_total * inv_root)
    gq = jnp.concatenate([gq_t[:, h * TR:(h + 1) * TR].T for h in range(H)], axis=1).astype(BF16)
    bands = [slice(i * (D // 2), (i + 1) * (D // 2)) for i in range(2)]
    pt_put = []
    for i, band in enumerate(bands):
        pulled = dot(gq, wq[band, :], NT)
        if RR % 8:
            wide_stage[...] = pulled
        for place in range(T):
            rows = slice(place * RR, (place + 1) * RR)
            block = wide_stage[rows, :] if RR % 8 else pulled[rows]
            pt[place % CORES, i, place // CORES] = block.astype(BF16)
        pt_put.append(put(pt.at[1 - c, i], pt_in.at[i], sibling))
    settle(order[0])
    for d in near:
        att_put[d].append(put(att.at[0, bottom], att.at[d, bottom], sp_peer(d)))
    backward(order[1])
    z_order = sorted(range(1, Z), key=lambda d: (abs(Z // 2 - d), d))
    ptr_put = {d: [] for d in z_order}
    for i in range(2):
        pt_put[i].wait_recv()
        ptr[i] = (pt[c, i].astype(F32) + pt_in[i].astype(F32)).astype(BF16)
        for d in z_order:
            ptr_put[d].append(put(ptr.at[i, lax.rem(z + d, Z)], ptr_in.at[i, d], z_peer(d)))
    for before, d in zip(order[1:], order[2:]):
        backward(d)
        settle(before)
    settle(0)
    for d in far:
        att_put[d].append(put(att.at[0], att.at[d], sp_peer(d)))
    cot_fwd = [None]
    for d in range(1, S):
        cot_put[d].wait_recv()
        cot_fwd.append(put(cotb.at[d, c], cotb.at[d, c], sibling))

    fin_put = {}
    for n, j in enumerate(pieces):
        at = pl.ds(0, Z) if j is None else pl.ds(lax.rem(z + j, Z), 1)
        summed = red[0, at].astype(F32)
        for d in range(1, S):
            red_put[d][n].wait_recv()
            summed = summed + red_in[d, at].astype(F32)
        red2[at] = summed.astype(BF16)
        for d in z_order if j is None else [j] if j else []:
            fin_put[d] = put(red2.at[lax.rem(z + d, Z)], fin_in.at[d], z_peer(d))

    ups = []
    for i in range(2):
        up = ptr[i, z].astype(F32)
        for d in z_order:
            ptr_put[d][i].wait_recv()
            up = up + ptr_in[i, d].astype(F32)
        ups.append(up)
    up = jnp.concatenate(ups, axis=1)
    gt_ref[...] = norm_back(own_rows(target, t, RR), tgain[...], up).astype(BF16)

    def go_part(places):
        rows, lefts = [], []
        for d in places:
            if d:
                for copy in att_put[d]:
                    copy.wait_recv()
                cot_fwd[d].wait_recv()
                rows.append(jnp.concatenate([cotb[d, 0], cotb[d, 1]], axis=0))
            else:
                rows.append(cot[:, pl.ds(pl.multiple_of(me * W, 128), W)])
            lefts.append(att[d])
        right = jnp.concatenate(rows, axis=0)
        return [
            dot(jnp.concatenate([a[:, h * TR:(h + 1) * TR] for a in lefts], axis=1), right)
            for h in range(H)
        ]

    first, second = go_part(range(S // 2)), go_part(range(S // 2, S))
    for h in range(H):
        go_ref[h * HEAD:(h + 1) * HEAD, :] = (first[h] + second[h]).astype(BF16)

    last = red2[z].astype(F32)
    for d in z_order:
        fin_put[d].wait_recv()
        last = last + fin_in[d].astype(F32)
    up = dot(last.astype(BF16), wkv[...], NT)
    gs_ref[...] = norm_back(own_rows(source, t, SR), sgain[...], up).astype(BF16)
    for copy in sends:
        copy.wait_send()


def on_device(S, T, target, source, cotangent, target_gain, source_gain, w_query, w_key, w_value, w_out):
    TR, D = target.shape
    SG = source.shape[0]
    QW = w_query.shape[1]
    R = QW // HEAD * TR
    Z = T // CORES
    SR, RR, W = SG // T, TR // T, D // S
    N = 3 * (S - 1) + 3 * (S - 1) + 2 * (S - 1) + (S - 1) + S + 4 * (S - 1) + 3 * Z + 5
    hbm = pl.BlockSpec(memory_space=pltpu.HBM)
    vmem = pl.BlockSpec(memory_space=pltpu.VMEM)
    V = pltpu.VMEM
    results = pl.pallas_call(
        functools.partial(kernel, S, T),
        out_shape=(
            V((RR, D), BF16), V((SR, D), BF16), V((QW, W), BF16),
        ),
        in_specs=[hbm] * 9,
        out_specs=(vmem, vmem, vmem),
        scratch_shapes=[
            V((TR, D), BF16), V((SG, D), BF16), V((TR, D), BF16), V((1, D), F32), V((1, D), F32),
            V((D, QW), BF16), V((D, 2 * HEAD), BF16), V((QW, D), BF16),
            V((max(SG, TR), D), BF16),
            V((S, 2, SG // 2, 2 * HEAD), BF16), V((S, 2, TR // 2, W), BF16),
            V((S, HEAD, R), BF16), V((S, 2, SG // 2, R), F32), V((S, 2, SG // 2, R), F32),
            V((CORES, S, Z, SR, 2 * HEAD), BF16), V((S, Z, SR, 2 * HEAD), BF16),
            V((S, Z, SR, 2 * HEAD), BF16), V((S, Z, SR, 2 * HEAD), BF16),
            V((Z, SR, 2 * HEAD), BF16), V((Z, SR, 2 * HEAD), BF16),
            V((CORES, 2, Z, RR, D // 2), BF16), V((2, Z, RR, D // 2), BF16),
            V((2, Z, RR, D // 2), BF16), V((2, Z, RR, D // 2), BF16),
            V((SG, 2 * HEAD), F32), V((TR, D // 2) if RR % 8 else (8, 128), F32),
            pltpu.SemaphoreType.DMA((12,)),
            pltpu.SemaphoreType.DMA((N,)),
            pltpu.SemaphoreType.DMA((N,)),
        ],
        compiler_params=pltpu.CompilerParams(
            collective_id=0, has_side_effects=True, vmem_limit_bytes=60 * 1024 * 1024
        ),
        name="attn_back",
    )(
        target, source, cotangent, target_gain.reshape(1, D), source_gain.reshape(1, D),
        w_query, w_key, w_value, w_out,
    )
    return pl.pallas_call(
        put_out,
        out_shape=tuple(jax.ShapeDtypeStruct(r.shape, r.dtype) for r in results),
        in_specs=[vmem, vmem, vmem],
        out_specs=(hbm, hbm, hbm),
        scratch_shapes=[pltpu.SemaphoreType.DMA((3,))],
        compiler_params=pltpu.CompilerParams(vmem_limit_bytes=60 * 1024 * 1024),
        name="put_out",
    )(*[pltpu.with_memory_space_constraint(r, pltpu.VMEM) for r in results])


def put_out(a, b, c, a_out, b_out, c_out, sem):
    outs = [
        pltpu.make_async_copy(x, y, sem.at[i])
        for i, (x, y) in enumerate(((a, a_out), (b, b_out), (c, c_out)))
    ]
    for copy in outs:
        copy.start()
    for copy in outs:
        copy.wait()


def solution(mesh):
    in_specs = (
        P("sp", None), P("sp", None), P("sp", None), P(), P(),
        P(None, "tp"), P(), P(), P("tp", None),
    )
    out_specs = (P(("sp", "tp"), None), P(("sp", "tp"), None), P("tp", "sp"))
    return jax.shard_map(
        functools.partial(on_device, mesh.shape["sp"], mesh.shape["tp"]),
        mesh=mesh, in_specs=in_specs, out_specs=out_specs, check_vma=False,
    )
```

time: 34.9 us -> 29.9 us (0.86)
  Pallas kernels: 34 us -> 29.1 us
    pallas_call x1, Pallas kernels: 32 us -> 28.2 us  [on_device(): pl.pallas_call(functools.partial(kernel, S, T), out_shape=(V((RR, D), BF1...]
    pallas_call x1, Pallas kernels: 2.02 us -> 0.91 us  [on_device(): pl.pallas_call(put_out, out_shape=tuple((jax.ShapeDtypeStruct(r.shape, r....]
where the time goes in v1:
time: 29.9 us; the launch traced here: 29.7 us
  Pallas kernels  29.1 us (97%)
  between operations  0.64 us (2%)
    pallas_call x1, Pallas kernels, on_device(): pl.pallas_call(functools.partial(kernel, S, T), out_shape=(V((RR, D), BF1...  28.2 us
    pallas_call x1, Pallas kernels, on_device(): pl.pallas_call(put_out, out_shape=tuple((jax.ShapeDtypeStruct(r.shape, r....  0.91 us

profile of v1, /device:TPU:0, one launch (start us, length us, event | category | flops | bytes accessed | tf_op | source)
XLA Modules:
  0.0 29.7 jit_solution(5218285347589271004)
XLA Ops:
  0.6 28.2 %attn_back.1 = (bf16[16,2048]{1,0:T(8,128)(2,1)S(1)}, bf16[48,2048]{1,0:T(8,128)(2,1)S(1)}, bf16[512,512]{1,0:T(8,128)(2,1)S(1)}) custom-call(bf16[128,2048]{1,0:T(8,128)(2,1)} %target_h.1, bf16[384,2048]{1,0:T(8,128)(2,1)} %source_h.1, bf16[128,2048]{1,0:T(8,128)(2,1)} %cot_h.1, f32[1,2048]{1,0:T(1,128)} %bitcast.2, f32[1,2048]{1,0:T(1,128)} %bitcast.3, ...), custom_call_target="tpu_custom_call" | custom-call | tf_op jit(solution)/shard_map/attn_back/pallas_call | solution.py:345
  28.8 0.9 %put_out.1 = (bf16[16,2048]{1,0:T(8,128)(2,1)}, bf16[48,2048]{1,0:T(8,128)(2,1)}, bf16[512,512]{1,0:T(8,128)(2,1)}) custom-call(bf16[16,2048]{1,0:T(8,128)(2,1)S(1)} %get-tuple-element.6.a, bf16[48,2048]{1,0:T(8,128)(2,1)S(1)} %get-tuple-element.7.b, bf16[512,512]{1,0:T(8,128)(2,1)S(1)} %get-tuple-element.8.c), custom_call_target="tpu_custom_call" | custom-call | tf_op jit(solution)/shard_map/put_out/pallas_call | solution.py:376

commit v2 on v1

--- a/solution.py
+++ b/solution.py
@@ -41,9 +41,12 @@
     return lax.rsqrt(jnp.sum(squares, axis=1, keepdims=True) * (1.0 / D) + NORM_EPS)
 
 
-def norm_back(wide, gain, upstream):
+def unit_of(wide):
     inv = inv_rms_of(wide)
-    unit = wide * inv
+    return inv, wide * inv
+
+
+def norm_back(inv, unit, gain, upstream):
     pulled = upstream * gain
     return inv * (pulled - unit * jnp.mean(pulled * unit, axis=1, keepdims=True))
 
@@ -63,7 +66,7 @@
     target_h, source_h, cot_h, tgain_h, sgain_h, wq_h, wk_h, wv_h, wo_h,
     gt_ref, gs_ref, go_ref,
     target, source, cot, tgain, sgain, wq, wkv, wo, normed, kv, cotb, att, e_buf, pg_buf,
-    kvg, kvg_in, red, red_in, red2, fin_in, pt, pt_in, ptr, ptr_in, stage, wide_stage,
+    kvg, kvg_in, red, red_in, red2, fin_in, pt, pt_in, ptr, ptr_in, pt_out, stage, wide_stage,
     load_sem, send, recv,
 ):
     Z = T // CORES
@@ -102,10 +105,15 @@
     def z_peer(d):
         return {"sp": me, "tp": lax.rem(z + d, Z) * CORES + c}
 
-    sends = []
+    twin_z = z + 1 - 2 * lax.rem(z, 2)
+    twin = {"sp": me, "tp": twin_z * CORES + c}
+    rest = pl.ds(1, S - 1)
+
+    sends, lanes = [], []
 
     def put(src, dst, who):
-        lane = len(sends)
+        lane = len(lanes)
+        lanes.append(lane)
         copy = pltpu.make_async_remote_copy(
             src_ref=src, dst_ref=dst, send_sem=send.at[lane], recv_sem=recv.at[lane],
             device_id=who, device_id_type=MESH,
@@ -113,6 +121,11 @@
         copy.start()
         sends.append(copy)
         return copy
+
+    def gone(copies):
+        for copy in copies:
+            copy.wait_send()
+            sends[:] = [other for other in sends if other is not copy]
 
     def own_half(i):
         return pl.ds(pl.multiple_of(c * half + i * chunk, chunk), chunk)
@@ -125,7 +138,7 @@
         (source_h.at[others], source.at[others]),
     ] + [(source_h.at[own_half(i)], source.at[own_half(i)]) for i in range(1, parts)]
     loads = [pltpu.make_async_copy(a, b, load_sem.at[i]) for i, (a, b) in enumerate(pairs)]
-    for i in (0, 1, 2, 3, *range(10, 9 + parts)):
+    for i in (0, 1, 2, 3):
         loads[i].start()
 
     barrier = pltpu.get_barrier_semaphore()
@@ -138,7 +151,7 @@
         if i == 0:
             loads[0].wait()
             loads[1].wait()
-            for j in (5, 4, 7, 6, 8, 9):
+            for j in (*range(10, 9 + parts), 5, 4, 7, 6, 8, 9):
                 loads[j].start()
         else:
             loads[9 + i].wait()
@@ -162,52 +175,59 @@
     loads[8].wait()
     grad = dot(cot[...], wo[...], NT)
     split = [slice(h * HEAD, (h + 1) * HEAD) for h in range(H)]
+    split_rows = [slice(h * TR, (h + 1) * TR) for h in range(H)]
     q_rows = jnp.concatenate([query[:, h] for h in split], axis=0).astype(BF16)
     g_rows = jnp.concatenate([grad[:, h] for h in split], axis=0).astype(BF16)
     q_cols = jnp.concatenate([query[:, h].T for h in split], axis=1).astype(BF16)
     g_cols = jnp.concatenate([grad[:, h].T for h in split], axis=1).astype(BF16)
 
     def forward(blocks):
-        both = jnp.concatenate([kv[d, part] for d, part in blocks], axis=0)
+        both = jnp.concatenate([kv[block] for block in blocks], axis=0)
         k, v = both[:, :HEAD], both[:, HEAD:]
         e = jnp.exp2(dot(k, q_cols) * (inv_root * math.log2(math.e)))
         prob_grad = dot(v, g_cols)
-        for i, (d, part) in enumerate(blocks):
-            e_buf[d, part] = e[i * half:(i + 1) * half]
-            pg_buf[d, part] = prob_grad[i * half:(i + 1) * half]
+        at = 0
+        for block in blocks:
+            count = block[2].size
+            e_buf[block] = e[at:at + count]
+            pg_buf[block] = prob_grad[at:at + count]
+            at += count
         tilted = (e * prob_grad).astype(BF16)
         return jnp.sum(e, axis=0, keepdims=True), dot(both, e.astype(BF16), TN), dot(k, tilted, TN)
 
     def more(state, blocks):
         return tuple(a + b for a, b in zip(state, forward(blocks)))
 
-    kv_fwd = {}
-
-    def hand_on(places):
-        for d in places:
-            for copy in kv_put[d]:
-                copy.wait_recv()
-            kv_fwd[d] = put(kv.at[d, c], kv.at[d, c], sibling)
-
     loads[9].wait()
     kv_twin.wait_recv()
-    state = forward([(0, c), (0, 1 - c)])
-    hand_on(near + far)
-    cot_put = [None]
-    for d in range(1, S):
-        columns = pl.ds(pl.multiple_of(sp_place(d) * W, 128), W)
-        rows = pl.ds(pl.multiple_of(c * thalf, thalf), thalf)
-        cot_put.append(put(cot.at[rows, columns], cotb.at[d, c], sp_peer(d)))
-
-    state = more(state, [(d, c) for d in near + far])
-    for d in near + far:
-        kv_fwd[d].wait_recv()
-    state = more(state, [(d, 1 - c) for d in near + far])
+    chunks = [pl.ds(i * chunk, chunk) for i in range(parts)]
+    state = forward([(0, part, rows) for part in (c, 1 - c) for rows in chunks])
+    kv_fwd = []
+    cot_put = []
+    held = []
+    for i, rows in enumerate(chunks):
+        for d in near + far:
+            kv_put[d][i].wait_recv()
+            kv_fwd.append(put(kv.at[d, c, rows], kv.at[d, c, rows], sibling))
+        if i:
+            for copy in kv_fwd[(i - 1) * (S - 1):i * (S - 1)]:
+                copy.wait_recv()
+        state = more(state, [(d, c, rows) for d in near + far] + held)
+        held = [(d, 1 - c, rows) for d in near + far]
+        if i == 0:
+            gone([copy for d in kv_put for copy in kv_put[d]])
+            lines = pl.ds(pl.multiple_of(c * thalf, thalf), thalf)
+            for d in range(1, S):
+                columns = pl.ds(pl.multiple_of(sp_place(d) * W, 128), W)
+                cot_put.append(put(cot.at[lines, columns], cotb.at[d, c], sp_peer(d)))
+    for copy in kv_fwd[-(S - 1):]:
+        copy.wait_recv()
+    state = more(state, held)
     total, weighted, tilted_sum = state
     inv_total = 1.0 / total
     att_t = (weighted[HEAD:] * inv_total).astype(BF16)
     att[0] = att_t
-    top, bottom = pl.ds(0, HEAD // 2), pl.ds(HEAD // 2, HEAD // 2)
+    top, bottom = pl.ds(0, HEAD * 5 // 8), pl.ds(HEAD * 5 // 8, HEAD * 3 // 8)
     att_put = {d: [] for d in range(1, S)}
     for d in near:
         att_put[d].append(put(att.at[0, top], att.at[d, top], sp_peer(d)))
@@ -243,13 +263,13 @@
                 red_put[d].append(put(red.at[d, at], red_in.at[d, at], sp_peer(d, -1)))
 
     order = list(range(S - 1, -1, -1))
-    backward(order[0])
-    gq_t = (tilted_sum - delta * weighted[:HEAD]) * (inv_total * inv_root)
-    gq = jnp.concatenate([gq_t[:, h * TR:(h + 1) * TR].T for h in range(H)], axis=1).astype(BF16)
-    bands = [slice(i * (D // 2), (i + 1) * (D // 2)) for i in range(2)]
+    z_order = sorted(range(1, Z), key=lambda d: (abs(Z // 2 - d), d))
     pt_put = []
-    for i, band in enumerate(bands):
-        pulled = dot(gq, wq[band, :], NT)
+    ptr_put = [[], []]
+    relayed = [0] if Z == 4 else []
+
+    def pull(i):
+        pulled = dot(gq, wq[bands[i], :], NT)
         if RR % 8:
             wide_stage[...] = pulled
         for place in range(T):
@@ -257,28 +277,56 @@
             block = wide_stage[rows, :] if RR % 8 else pulled[rows]
             pt[place % CORES, i, place // CORES] = block.astype(BF16)
         pt_put.append(put(pt.at[1 - c, i], pt_in.at[i], sibling))
+
+    def send_pulled(i):
+        pt_put[i].wait_recv()
+        ptr[i] = (pt[c, i].astype(F32) + pt_in[i].astype(F32)).astype(BF16)
+        if i in relayed:
+            ptr_put[i].append(put(ptr.at[i, lax.rem(twin_z + 2, Z)], ptr_in.at[i, 0], twin))
+            ptr_put[i].append(put(ptr.at[i, twin_z], ptr_in.at[i, 1], twin))
+        else:
+            for d in z_order:
+                ptr_put[i].append(put(ptr.at[i, lax.rem(z + d, Z)], ptr_in.at[i, d], z_peer(d)))
+
+    def relay_pulled(i):
+        ptr_put[i].pop(0).wait_recv()
+        across = lax.rem(z + 2, Z)
+        pt_out[...] = (ptr[i, across].astype(F32) + ptr_in[i, 0].astype(F32)).astype(BF16)
+        ptr_put[i].append(put(pt_out, ptr_in.at[i, 2], z_peer(2)))
+
+    backward(order[0])
+    gq_t = (tilted_sum - delta * weighted[:HEAD]) * (inv_total * inv_root)
+    gq = jnp.concatenate([gq_t[:, h].T for h in split_rows], axis=1).astype(BF16)
+    bands = [slice(i * (D // 2), (i + 1) * (D // 2)) for i in range(2)]
+    pull(0)
+    backward(order[1])
     settle(order[0])
+    pull(1)
+    for copy in cot_put:
+        copy.wait_recv()
+    for i, d in enumerate(order[2:]):
+        backward(d)
+        if i < 2:
+            send_pulled(i)
+        settle(order[i + 1])
+    for i in range(S - 2, 2):
+        send_pulled(i)
+    settle(0)
+    for i in relayed:
+        relay_pulled(i)
+    for d in near:
+        att_put[d][0].wait_recv()
+    for d in far:
+        dy, dx = steps[d]
+        side = steps.index((0, dx))
+        att_put[d].append(put(att.at[0, bottom], att.at[d, bottom], sp_peer(d)))
+        att_put[d].append(put(att.at[side, top], att.at[d, top], sp_peer(steps.index((dy, 0)))))
     for d in near:
         att_put[d].append(put(att.at[0, bottom], att.at[d, bottom], sp_peer(d)))
-    backward(order[1])
-    z_order = sorted(range(1, Z), key=lambda d: (abs(Z // 2 - d), d))
-    ptr_put = {d: [] for d in z_order}
-    for i in range(2):
-        pt_put[i].wait_recv()
-        ptr[i] = (pt[c, i].astype(F32) + pt_in[i].astype(F32)).astype(BF16)
-        for d in z_order:
-            ptr_put[d].append(put(ptr.at[i, lax.rem(z + d, Z)], ptr_in.at[i, d], z_peer(d)))
-    for before, d in zip(order[1:], order[2:]):
-        backward(d)
-        settle(before)
-    settle(0)
-    for d in far:
-        att_put[d].append(put(att.at[0], att.at[d], sp_peer(d)))
-    cot_fwd = [None]
-    for d in range(1, S):
-        cot_put[d].wait_recv()
-        cot_fwd.append(put(cotb.at[d, c], cotb.at[d, c], sibling))
-
+    cot_fwd = put(cotb.at[rest, c], cotb.at[rest, c], sibling)
+
+    target_unit = unit_of(own_rows(target, t, RR))
+    source_unit = unit_of(own_rows(source, t, SR))
     fin_put = {}
     for n, j in enumerate(pieces):
         at = pl.ds(0, Z) if j is None else pl.ds(lax.rem(z + j, Z), 1)
@@ -292,22 +340,22 @@
 
     ups = []
     for i in range(2):
+        for copy in ptr_put[i]:
+            copy.wait_recv()
         up = ptr[i, z].astype(F32)
-        for d in z_order:
-            ptr_put[d][i].wait_recv()
+        for d in (1, 2) if i in relayed else z_order:
             up = up + ptr_in[i, d].astype(F32)
         ups.append(up)
     up = jnp.concatenate(ups, axis=1)
-    gt_ref[...] = norm_back(own_rows(target, t, RR), tgain[...], up).astype(BF16)
+    gt_ref[...] = norm_back(*target_unit, tgain[...], up).astype(BF16)
 
     def go_part(places):
         rows, lefts = [], []
         for d in places:
             if d:
-                for copy in att_put[d]:
+                for copy in att_put[d][1 if d in near else 0:]:
                     copy.wait_recv()
-                cot_fwd[d].wait_recv()
-                rows.append(jnp.concatenate([cotb[d, 0], cotb[d, 1]], axis=0))
+                rows.append(cotb[d].reshape(TR, W))
             else:
                 rows.append(cot[:, pl.ds(pl.multiple_of(me * W, 128), W)])
             lefts.append(att[d])
@@ -317,16 +365,17 @@
             for h in range(H)
         ]
 
-    first, second = go_part(range(S // 2)), go_part(range(S // 2, S))
-    for h in range(H):
-        go_ref[h * HEAD:(h + 1) * HEAD, :] = (first[h] + second[h]).astype(BF16)
-
+    cot_fwd.wait_recv()
+    first = go_part(range(S // 2))
     last = red2[z].astype(F32)
     for d in z_order:
         fin_put[d].wait_recv()
         last = last + fin_in[d].astype(F32)
     up = dot(last.astype(BF16), wkv[...], NT)
-    gs_ref[...] = norm_back(own_rows(source, t, SR), sgain[...], up).astype(BF16)
+    gs_ref[...] = norm_back(*source_unit, sgain[...], up).astype(BF16)
+    second = go_part(range(S // 2, S))
+    for h in range(H):
+        go_ref[h * HEAD:(h + 1) * HEAD, :] = (first[h] + second[h]).astype(BF16)
     for copy in sends:
         copy.wait_send()
 
@@ -359,7 +408,7 @@
             V((S, Z, SR, 2 * HEAD), BF16), V((S, Z, SR, 2 * HEAD), BF16),
             V((Z, SR, 2 * HEAD), BF16), V((Z, SR, 2 * HEAD), BF16),
             V((CORES, 2, Z, RR, D // 2), BF16), V((2, Z, RR, D // 2), BF16),
-            V((2, Z, RR, D // 2), BF16), V((2, Z, RR, D // 2), BF16),
+            V((2, Z, RR, D // 2), BF16), V((2, Z, RR, D // 2), BF16), V((RR, D // 2), BF16),
             V((SG, 2 * HEAD), F32), V((TR, D // 2) if RR % 8 else (8, 128), F32),
             pltpu.SemaphoreType.DMA((12,)),
             pltpu.SemaphoreType.DMA((N,)),

time: 29.9 us -> 29.1 us (0.973)
  Pallas kernels: 29.1 us -> 28.3 us
    pallas_call x1, Pallas kernels: 28.2 us -> 27.4 us  [on_device(): pl.pallas_call(functools.partial(kernel, S, T), out_shape=(V((RR, D), BF1...]
where the time goes in v2:
time: 29.1 us; the launch traced here: 28.9 us
  Pallas kernels  28.3 us (97%)
  between operations  0.64 us (2%)
    pallas_call x1, Pallas kernels, on_device(): pl.pallas_call(functools.partial(kernel, S, T), out_shape=(V((RR, D), BF1...  27.4 us
    pallas_call x1, Pallas kernels, on_device(): pl.pallas_call(put_out, out_shape=tuple((jax.ShapeDtypeStruct(r.shape, r....  0.91 us

profile of v2, /device:TPU:0, one launch (start us, length us, event | category | flops | bytes accessed | tf_op | source)
XLA Modules:
  0.0 28.9 jit_solution(517736649171464762)
XLA Ops:
  0.6 27.4 %attn_back.1 = (bf16[16,2048]{1,0:T(8,128)(2,1)S(1)}, bf16[48,2048]{1,0:T(8,128)(2,1)S(1)}, bf16[512,512]{1,0:T(8,128)(2,1)S(1)}) custom-call(bf16[128,2048]{1,0:T(8,128)(2,1)} %target_h.1, bf16[384,2048]{1,0:T(8,128)(2,1)} %source_h.1, bf16[128,2048]{1,0:T(8,128)(2,1)} %cot_h.1, f32[1,2048]{1,0:T(1,128)} %bitcast.2, f32[1,2048]{1,0:T(1,128)} %bitcast.3, ...), custom_call_target="tpu_custom_call" | custom-call | tf_op jit(solution)/shard_map/attn_back/pallas_call | solution.py:394
  28.0 0.9 %put_out.1 = (bf16[16,2048]{1,0:T(8,128)(2,1)}, bf16[48,2048]{1,0:T(8,128)(2,1)}, bf16[512,512]{1,0:T(8,128)(2,1)}) custom-call(bf16[16,2048]{1,0:T(8,128)(2,1)S(1)} %get-tuple-element.6.a, bf16[48,2048]{1,0:T(8,128)(2,1)S(1)} %get-tuple-element.7.b, bf16[512,512]{1,0:T(8,128)(2,1)S(1)} %get-tuple-element.8.c), custom_call_target="tpu_custom_call" | custom-call | tf_op jit(solution)/shard_map/put_out/pallas_call | solution.py:425

commit v3 on v2

--- a/solution.py
+++ b/solution.py
@@ -138,7 +138,7 @@
         (source_h.at[others], source.at[others]),
     ] + [(source_h.at[own_half(i)], source.at[own_half(i)]) for i in range(1, parts)]
     loads = [pltpu.make_async_copy(a, b, load_sem.at[i]) for i, (a, b) in enumerate(pairs)]
-    for i in (0, 1, 2, 3):
+    for i in (2, 3, 1, 0):
         loads[i].start()
 
     barrier = pltpu.get_barrier_semaphore()
@@ -312,6 +312,8 @@
     for i in range(S - 2, 2):
         send_pulled(i)
     settle(0)
+    for d in far + near:
+        att_put[d].append(put(att.at[0, bottom], att.at[d, bottom], sp_peer(d)))
     for i in relayed:
         relay_pulled(i)
     for d in near:
@@ -319,10 +321,7 @@
     for d in far:
         dy, dx = steps[d]
         side = steps.index((0, dx))
-        att_put[d].append(put(att.at[0, bottom], att.at[d, bottom], sp_peer(d)))
         att_put[d].append(put(att.at[side, top], att.at[d, top], sp_peer(steps.index((dy, 0)))))
-    for d in near:
-        att_put[d].append(put(att.at[0, bottom], att.at[d, bottom], sp_peer(d)))
     cot_fwd = put(cotb.at[rest, c], cotb.at[rest, c], sibling)
 
     target_unit = unit_of(own_rows(target, t, RR))

time: 29.1 us -> 29.1 us (level)
  no operation moved by 1% of the time
where the time goes in v3:
time: 29.1 us; the launch traced here: 28.9 us
  Pallas kernels  28.3 us (97%)
  between operations  0.64 us (2%)
    pallas_call x1, Pallas kernels, on_device(): pl.pallas_call(functools.partial(kernel, S, T), out_shape=(V((RR, D), BF1...  27.3 us
    pallas_call x1, Pallas kernels, on_device(): pl.pallas_call(put_out, out_shape=tuple((jax.ShapeDtypeStruct(r.shape, r....  0.91 us

profile of v3, /device:TPU:0, one launch (start us, length us, event | category | flops | bytes accessed | tf_op | source)
XLA Modules:
  0.0 28.9 jit_solution(40440759406635553)
XLA Ops:
  0.6 27.3 %attn_back.1 = (bf16[16,2048]{1,0:T(8,128)(2,1)S(1)}, bf16[48,2048]{1,0:T(8,128)(2,1)S(1)}, bf16[512,512]{1,0:T(8,128)(2,1)S(1)}) custom-call(bf16[128,2048]{1,0:T(8,128)(2,1)} %target_h.1, bf16[384,2048]{1,0:T(8,128)(2,1)} %source_h.1, bf16[128,2048]{1,0:T(8,128)(2,1)} %cot_h.1, f32[1,2048]{1,0:T(1,128)} %bitcast.2, f32[1,2048]{1,0:T(1,128)} %bitcast.3, ...), custom_call_target="tpu_custom_call" | custom-call | tf_op jit(solution)/shard_map/attn_back/pallas_call | solution.py:393
  28.0 0.9 %put_out.1 = (bf16[16,2048]{1,0:T(8,128)(2,1)}, bf16[48,2048]{1,0:T(8,128)(2,1)}, bf16[512,512]{1,0:T(8,128)(2,1)}) custom-call(bf16[16,2048]{1,0:T(8,128)(2,1)S(1)} %get-tuple-element.6.a, bf16[48,2048]{1,0:T(8,128)(2,1)S(1)} %get-tuple-element.7.b, bf16[512,512]{1,0:T(8,128)(2,1)S(1)} %get-tuple-element.8.c), custom_call_target="tpu_custom_call" | custom-call | tf_op jit(solution)/shard_map/put_out/pallas_call | solution.py:424
